TPU v7x, 32 devices: a whole 2x2x4 slice. The times are simulated.
32 devices in a mesh: sp: 8 (over z, x), tp: 4 (over y, core).
Axes of the slice: x: 2, y: 2, z: 4, core: 2. Of those that a mesh axis runs over, the one named last changes fastest.
Arguments:
- tokens: bfloat16 [2048, 2048], P(('sp', 'tp')), may hold values from -40 to 40
- w_query: bfloat16 [2048, 1024], P(None, 'tp'), may hold values from -0.125 to 0.125
- w_key: bfloat16 [2048, 256], P(None, 'tp'), may hold values from -0.125 to 0.125
- w_value: bfloat16 [2048, 256], P(None, 'tp'), may hold values from -0.125 to 0.125
- w_out: bfloat16 [1024, 2048], P('tp'), may hold values from -0.1875 to 0.1875
- cum_gate: float32 [16, 2048], P('tp', 'sp'), may hold values from -295 to 0, as said below
Outputs:
- layer_out: bfloat16 [2048, 2048], P(('sp', 'tp'))
Inputs may be any that keep to these rules, and one draw needn't show every extreme that they name: `cum_gate`: each head's row does not rise along the positions.
All inputs are finite; a program needn't handle non-finite values.
Results may differ from a plain program's by a relative error of at most 0.012.
Values may be sent and summed in bfloat16 or wider, within the bound.
A program may use at most 64 MiB of HBM per device.

v0:
```python
import math

import jax
import jax.numpy as jnp
from jax import lax
from jax.sharding import PartitionSpec as P

HD = 64


def per_device(tokens, w_query, w_key, w_value, w_out, cum_gate):
    pieces = lax.all_gather(tokens, "tp", axis=0, tiled=True)
    query_part = jnp.dot(pieces, w_query, preferred_element_type=jnp.float32).astype(jnp.bfloat16)
    key_part = jnp.dot(pieces, w_key, preferred_element_type=jnp.float32).astype(jnp.bfloat16)
    value_part = jnp.dot(pieces, w_value, preferred_element_type=jnp.float32).astype(jnp.bfloat16)
    projected = jnp.concatenate([query_part, key_part, value_part], axis=1)
    row_count = projected.shape[0]
    heads_local = w_query.shape[1] // HD
    kv_local = w_key.shape[1] // HD
    group_size = heads_local // kv_local
    score_factor = float(HD) ** (-0.5)
    query_flat = projected[:, : heads_local * HD]
    key_values = projected[:, heads_local * HD :]
    first_pos = lax.axis_index("sp") * row_count
    own_pos = first_pos + jnp.arange(row_count, dtype=jnp.int32)
    gate_all = lax.all_gather(cum_gate, "sp", axis=1, tiled=True)
    groups = (query_flat, cum_gate, own_pos)
    prepared = []
    query_rows, query_gates, query_pos = groups
    count = query_rows.shape[0]
    prepared.append(
        (
            query_rows.reshape(count, kv_local, group_size, HD),
            query_gates.reshape(kv_local, group_size, count, 1),
            query_pos,
            jnp.max(query_pos),
        )
    )
    initial = tuple(
        (
            (
                jnp.full((kv_local, group_size, member[2].shape[0]), -1e30, jnp.float32),
                jnp.zeros((kv_local, group_size, member[2].shape[0]), jnp.float32),
                jnp.zeros((kv_local, group_size, member[2].shape[0], HD), jnp.float32),
            )
            for member in prepared
        )
    )
    pieces = lax.all_gather(key_values, "sp", axis=0, tiled=True)
    piece_rows = pieces.shape[0]
    key_block = math.gcd(piece_rows, 1024)

    def one_block(index, hidden_vectors):
        block_start = index * key_block
        slab = lax.dynamic_slice_in_dim(pieces, block_start, key_block, 0)
        key_rows = slab[:, : kv_local * HD].reshape(key_block, kv_local, HD)
        value_rows = slab[:, kv_local * HD :].reshape(key_block, kv_local, HD)
        key_cum = lax.dynamic_slice_in_dim(gate_all, block_start, key_block, 1)
        key_cum = key_cum.reshape(kv_local, group_size, 1, key_block)
        key_pos = block_start + jnp.arange(key_block, dtype=jnp.int32)
        results = []
        for member, state in zip(prepared, hidden_vectors):
            queries, query_cum, query_pos, last_pos = member

            def compute(inner, queries=queries, query_cum=query_cum, query_pos=query_pos):
                top_score, weight_sum, accumulated = inner
                scores = (
                    jnp.einsum(
                        "tkgd,skd->kgts", queries, key_rows, preferred_element_type=jnp.float32
                    )
                    * score_factor
                )
                scores = scores + (query_cum - key_cum)
                scores = jnp.where(key_pos[None, :] <= query_pos[:, None], scores, -jnp.inf)
                new_top = jnp.maximum(top_score, jnp.max(scores, axis=-1))
                weights = jnp.exp(scores - new_top[..., None])
                decay = jnp.exp(top_score - new_top)
                weight_sum = weight_sum * decay + jnp.sum(weights, axis=-1)
                update = jnp.einsum(
                    "kgts,skd->kgtd",
                    weights.astype(jnp.bfloat16),
                    value_rows,
                    preferred_element_type=jnp.float32,
                )
                accumulated = accumulated * decay[..., None] + update
                return (new_top, weight_sum, accumulated)

            def skipped(inner):
                return inner

            results.append(lax.cond(block_start <= last_pos, compute, skipped, state))
        return tuple(results)

    finals = lax.fori_loop(0, piece_rows // key_block, one_block, initial)
    parts = []
    for top_score, weight_sum, accumulated in finals:
        count = weight_sum.shape[2]
        rows = (accumulated / weight_sum[..., None]).astype(jnp.bfloat16)
        parts.append(rows.transpose(2, 0, 1, 3).reshape(count, heads_local * HD))
    attended = parts[0]
    regrouped = lax.all_to_all(attended, "tp", split_axis=0, concat_axis=1, tiled=True)
    summed = jnp.dot(
        regrouped,
        lax.all_gather(w_out, "tp", axis=0, tiled=True),
        preferred_element_type=jnp.float32,
    )
    return summed.astype(jnp.bfloat16)


def solution(mesh):
    placed = (
        P(("sp", "tp"), None),
        P(None, "tp"),
        P(None, "tp"),
        P(None, "tp"),
        P("tp", None),
        P("tp", "sp"),
    )
    return jax.shard_map(
        per_device, mesh=mesh, in_specs=placed, out_specs=P(("sp", "tp"), None), check_vma=False
    )
```

profile of v0, /device:TPU:26, one launch (start us, length us, event | category | flops | bytes accessed | tf_op | source)
XLA Modules:
  0.0 111.5 jit_solution(12001325183075027937)
XLA Ops:
  6.5 0.0 copy-start
  6.5 0.0 copy-start.2
  6.5 0.0 all-gather.3.cloned.1.call-start
  6.5 0.7 all-gather.3.cloned.1.call-update
  7.3 0.0 all-gather.5.cloned.1.call-start
  7.3 0.7 all-gather.5.cloned.1.call-update
  8.0 0.7 add_reduce_fusion
  8.7 30.7 %all_gather.14 = f32[4,2048]{1,0:T(4,128)S(1)} all-gather(f32[4,256]{1,0:T(4,128)} %param.15), channel_id=1, replica_groups=mesh['sp'=8,'tp'=4] {'sp'}, dimensions={1}, use_global_device_ids=true | all-gather | bytes 36864 | tf_op jit(solution)/shard_map/all_gather | solution.py:26
  39.4 0.0 all-gather.3.cloned.1.call-done
  39.4 1.7 %convolution_convert_fusion.2 = bf16[256,64]{0,1:T(8,128)(2,1)S(1)} fusion(bf16[256,2048]{1,0:T(8,128)(2,1)} %all-gather.3.cloned.1.call-done, bf16[2048,64]{0,1:T(8,128)(2,1)} %param.13), kind=kOutput, calls=%fused_computation.29 | convolution fusion | flops 67125248 | bytes 1343488 | tf_op jit(solution)/shard_map/dot_general | solution.py:15
  41.2 1.7 %convolution_convert_fusion.3 = bf16[256,64]{0,1:T(8,128)(2,1)S(1)} fusion(bf16[256,2048]{1,0:T(8,128)(2,1)} %all-gather.3.cloned.1.call-done, bf16[2048,64]{0,1:T(8,128)(2,1)} %param.12), kind=kOutput, calls=%fused_computation.30 | convolution fusion | flops 67125248 | bytes 1343488 | tf_op jit(solution)/shard_map/dot_general | solution.py:14
  42.9 31.4 %all_gather.13 = bf16[2048,128]{0,1:T(8,128)(2,1)S(1)} all-gather(bf16[256,128]{0,1:T(8,128)(2,1)S(1)} %pad_maximum_fusion), channel_id=1, replica_groups=mesh['sp'=8,'tp'=4] {'sp'}, dimensions={0}, use_global_device_ids=true | all-gather | bytes 589824 | tf_op jit(solution)/shard_map/all_gather | solution.py:49
  74.2 0.0 copy-done
  74.2 1.7 %convolution_convert_fusion.1 = bf16[256,256]{0,1:T(8,128)(2,1)S(1)} fusion(bf16[256,2048]{1,0:T(8,128)(2,1)} %all-gather.3.cloned.1.call-done, bf16[2048,256]{1,0:T(8,128)(2,1)S(1)} %copy-done), kind=kOutput, calls=%fused_computation.28 | convolution fusion | flops 268500992 | bytes 2228224 | tf_op jit(solution)/shard_map/dot_general | solution.py:13
  76.0 0.0 copy-done.2
  76.1 17.2 %while.18 = (s32[]{:T(128)}, f32[1,4,256]{2,1,0:T(4,128)S(1)}, f32[1,4,256]{2,1,0:T(4,128)S(1)}, f32[1,4,256,64]{2,3,1,0:T(8,128)S(1)}, s32[]{:T(128)}, /*index=...) while((s32[]{:T(128)}, f32[1,4,256]{2,1,0:T(4,128)S(1)}, ...), condition=%wide.region_6.7_spmd.clone, body=%wide.region_1.6_spmd.clone.sunk | while | flops 286658816 | bytes 31506816 | solution.py:94
  76.8 7.9 %conditional.3 = ((f32[1,4,256]{2,1,0:T(4,128)S(1)}, f32[1,4,256]{2,1,0:T(4,128)S(1)}, f32[1,4,256,64]{2,3,1,0:T(8,128)S(1)})) conditional(s32[]{:T(128)} %convert_element_type.50, (f32[1,4,256]{2,1,0:T(4,128)S(1)}, f32[1,4,256]{2,1,0:T(4,128)S(1)}, f32[1,4,256,64]{2,3,1,0:T(8,128)S(1)}) %tuple.53, (s32[]{:T(128)}, s32[1024]{0:T(1024)S(1)}, ...), branch_computations={%region_2.0_spmd, %region_3.5_spmd} | conditional | flops 286658816 | bytes 31501442 | solution.py:91
  76.8 0.2 broadcast_compare_fusion
  77.0 2.7 %fusion.5 = (f32[4,256]{1,0:T(4,128)S(1)}, f32[1024,256,4]{1,0,2:T(8,128)}) fusion(f32[4,1024]{1,0:T(4,128)S(1)} %constant_dynamic-slice_fusion, f32[4,256]{1,0:T(4,128)S(1)} %bitcast.78, pred[256,1024]{0,1:T(8,128)(4,1)S(1)} %broadcast_compare_fusion, bf16[256,1,4,64]{0,3,2,1:T(8,128)(2,1)S(1)} %get-tuple-element.293, ...), kind=kOutput, calls=%fused_computation.6 | convolution fusion | flops 139459584 | bytes 4743172 | tf_op jit(solution)/shard_map/while/body/eval_jaxpr/cond/branch_1_fun/tkgd,skd->kgts/dot_general | solution.py:68
  79.7 0.0 copy-start.1
  79.7 3.5 %fusion.13 = f32[1,4,256,64]{2,3,1,0:T(8,128)S(1)} fusion(f32[1024,256,4]{1,0,2:T(8,128)} %get-tuple-element.368, f32[4,256]{1,0:T(4,128)S(1)} %bitcast.72, f32[4,1024]{1,0:T(4,128)S(1)} %constant_dynamic-slice_fusion, f32[4,256]{1,0:T(4,128)S(1)} %bitcast.79, pred[256,1024]{0,1:T(8,128)(4,1)S(1)} %broadcast_compare_fusion, ...), kind=kOutput, calls=%fused_computation.11 | convolution fusion | flops 140640256 | bytes 5140488 | tf_op jit(solution)/shard_map/while/body/eval_jaxpr/cond/branch_1_fun/kgts,skd->kgtd/dot_general | solution.py:79
  83.2 0.0 copy-done.1
  83.2 1.4 %fusion.4 = f32[4,256]{1,0:T(4,128)S(1)} fusion(f32[1024,256,4]{1,0,2:T(8,128)S(1)} %copy-done.1, f32[4,256]{1,0:T(4,128)S(1)} %bitcast.73, f32[4,1024]{1,0:T(4,128)S(1)} %constant_dynamic-slice_fusion, f32[4,256]{1,0:T(4,128)S(1)} %bitcast.80, pred[256,1024]{0,1:T(8,128)(4,1)S(1)} %broadcast_compare_fusion), kind=kLoop, calls=%fused_computation.5 | loop fusion | flops 6290432 | bytes 4485120 | tf_op jit(solution)/shard_map/while/body/eval_jaxpr/cond/branch_1_fun/reduce_sum | solution.py:78
  85.3 7.9 %conditional.3 = ((f32[1,4,256]{2,1,0:T(4,128)S(1)}, f32[1,4,256]{2,1,0:T(4,128)S(1)}, f32[1,4,256,64]{2,3,1,0:T(8,128)S(1)})) conditional(s32[]{:T(128)} %convert_element_type.50, (f32[1,4,256]{2,1,0:T(4,128)S(1)}, f32[1,4,256]{2,1,0:T(4,128)S(1)}, f32[1,4,256,64]{2,3,1,0:T(8,128)S(1)}) %tuple.53, (s32[]{:T(128)}, s32[1024]{0:T(1024)S(1)}, ...), branch_computations={%region_2.0_spmd, %region_3.5_spmd} | conditional | flops 286658816 | bytes 31501442 | solution.py:91
  85.4 0.2 broadcast_compare_fusion
  85.6 2.7 %fusion.5 = (f32[4,256]{1,0:T(4,128)S(1)}, f32[1024,256,4]{1,0,2:T(8,128)}) fusion(f32[4,1024]{1,0:T(4,128)S(1)} %constant_dynamic-slice_fusion, f32[4,256]{1,0:T(4,128)S(1)} %bitcast.78, pred[256,1024]{0,1:T(8,128)(4,1)S(1)} %broadcast_compare_fusion, bf16[256,1,4,64]{0,3,2,1:T(8,128)(2,1)S(1)} %get-tuple-element.293, ...), kind=kOutput, calls=%fused_computation.6 | convolution fusion | flops 139459584 | bytes 4743172 | tf_op jit(solution)/shard_map/while/body/eval_jaxpr/cond/branch_1_fun/tkgd,skd->kgts/dot_general | solution.py:68
  88.3 0.0 copy-start.1
  88.3 3.5 %fusion.13 = f32[1,4,256,64]{2,3,1,0:T(8,128)S(1)} fusion(f32[1024,256,4]{1,0,2:T(8,128)} %get-tuple-element.368, f32[4,256]{1,0:T(4,128)S(1)} %bitcast.72, f32[4,1024]{1,0:T(4,128)S(1)} %constant_dynamic-slice_fusion, f32[4,256]{1,0:T(4,128)S(1)} %bitcast.79, pred[256,1024]{0,1:T(8,128)(4,1)S(1)} %broadcast_compare_fusion, ...), kind=kOutput, calls=%fused_computation.11 | convolution fusion | flops 140640256 | bytes 5140488 | tf_op jit(solution)/shard_map/while/body/eval_jaxpr/cond/branch_1_fun/kgts,skd->kgtd/dot_general | solution.py:79
  91.8 0.0 copy-done.1
  91.8 1.4 %fusion.4 = f32[4,256]{1,0:T(4,128)S(1)} fusion(f32[1024,256,4]{1,0,2:T(8,128)S(1)} %copy-done.1, f32[4,256]{1,0:T(4,128)S(1)} %bitcast.73, f32[4,1024]{1,0:T(4,128)S(1)} %constant_dynamic-slice_fusion, f32[4,256]{1,0:T(4,128)S(1)} %bitcast.80, pred[256,1024]{0,1:T(8,128)(4,1)S(1)} %broadcast_compare_fusion), kind=kLoop, calls=%fused_computation.5 | loop fusion | flops 6290432 | bytes 4485120 | tf_op jit(solution)/shard_map/while/body/eval_jaxpr/cond/branch_1_fun/reduce_sum | solution.py:78
  93.3 0.2 reshape.96
  93.4 0.2 copy.12
  93.6 7.3 %all_to_all.19 = bf16[4,64,256]{2,1,0:T(8,128)(2,1)S(1)} all-to-all(bf16[4,64,256]{2,1,0:T(8,128)(2,1)S(1)} %copy.12), channel_id=1, replica_groups=mesh['sp'=8,'tp'=4] {'tp'}, dimensions={0} | all-to-all | bytes 262144 | tf_op jit(solution)/shard_map/all_to_all | solution.py:101
  100.9 0.0 all-gather.5.cloned.1.call-done
  100.9 3.7 %convolution_convert_fusion = bf16[64,2048]{1,0:T(8,128)(2,1)} fusion(bf16[64,1024]{1,0:T(8,128)(2,1)S(1)} %bitcast.74, bf16[1024,2048]{1,0:T(8,128)(2,1)} %all-gather.5.cloned.1.call-done), kind=kOutput, calls=%fused_computation.27 | convolution fusion | flops 268566528 | bytes 4587520 | tf_op jit(solution)/shard_map/dot_general | solution.py:102
  (22 shorter events, 0.2 us)
Async XLA Ops:
  6.5 67.7 %copy-start = (bf16[2048,256]{1,0:T(8,128)(2,1)S(1)}, bf16[2048,256]{1,0:T(8,128)(2,1)}, u32[]{:S(2)}) copy-start(bf16[2048,256]{1,0:T(8,128)(2,1)} %param.11) | copy-start | bytes 3145732
  6.5 69.5 %copy-start.2 = (f32[4,256]{1,0:T(4,128)S(1)}, f32[4,256]{1,0:T(4,128)}, u32[]{:S(2)}) copy-start(f32[4,256]{1,0:T(4,128)} %param.15) | copy-start | bytes 12292
  6.5 32.9 %all-gather.3.cloned.1.call-start = ((), (), s32[]{:S(2)}) async-start(), calls=%async_computation.1 | async-start | bytes 1310720 | tf_op jit(solution)/shard_map/all_gather | solution.py:12
  7.3 93.6 %all-gather.5.cloned.1.call-start = ((), (), s32[]{:S(2)}) async-start(), calls=%async_computation.2 | async-start | bytes 5242880 | tf_op jit(solution)/shard_map/all_gather | solution.py:104
  79.7 3.5 %copy-start.1 = (f32[1024,256,4]{1,0,2:T(8,128)S(1)}, f32[1024,256,4]{1,0,2:T(8,128)}, u32[]{:S(2)}) copy-start(f32[1024,256,4]{1,0,2:T(8,128)} %get-tuple-element.368) | copy-start | bytes 12582916 | tf_op jit(solution)/shard_map/while/body/eval_jaxpr/cond
  88.3 3.5 %copy-start.1 = (f32[1024,256,4]{1,0,2:T(8,128)S(1)}, f32[1024,256,4]{1,0,2:T(8,128)}, u32[]{:S(2)}) copy-start(f32[1024,256,4]{1,0,2:T(8,128)} %get-tuple-element.368) | copy-start | bytes 12582916 | tf_op jit(solution)/shard_map/while/body/eval_jaxpr/cond
Sparse Core Ops, SparseCore 0:
  8.9 17.6 all-gather.2
  28.1 34.4 all-gather.4
where the time goes:
time: 112 us; the launch traced here: 111 us
  blocking collectives  69.4 us (62%)
  matrix products  21.2 us (19%)
  between operations  13.5 us (12%)
  other arithmetic  3.96 us (4%)
  loops' own time  1.6 us (1%)
  waiting for transfers between devices  1.43 us (1%)
    all_gather x1, blocking collectives, per_device(): pieces = lax.all_gather(key_values, 'sp', axis=0, tiled=True)  31.4 us
    all_gather x1, blocking collectives, per_device(): gate_all = lax.all_gather(cum_gate, 'sp', axis=1, tiled=True)  30.7 us
    all_to_all x1, blocking collectives, per_device(): lax.all_to_all(attended, 'tp', split_axis=0, concat_axis=1, tiled=True)  7.26 us
    dot_general x2, matrix products, compute(): jnp.einsum('kgts,skd->kgtd', weights.astype(jnp.bfloat16), value_rows, pr...  6.97 us
    dot_general x2, matrix products, compute(): jnp.einsum('tkgd,skd->kgts', queries, key_rows, preferred_element_type=jn...  5.33 us
    dot_general x1, matrix products, per_device(): jnp.dot(regrouped, lax.all_gather(w_out, 'tp', axis=0, tiled=True), prefe...  3.74 us
    reduce_sum x2, other arithmetic, compute(): weight_sum = weight_sum * decay + jnp.sum(weights, axis=-1)  2.74 us
  transfers between devices with their start and end apart: 2, of which 0 were waited for; matrix products, arithmetic and copies ran while one was open for 20% of the time, Pallas kernels for 0%

commit v1 on v0

v1 whole, which is shorter than its diff:
```python
import functools

import jax
import jax.numpy as jnp
from jax import lax
from jax.experimental import pallas as pl
from jax.experimental.pallas import tpu as pltpu
from jax.sharding import PartitionSpec as P

HD = 64
MESH = pl.DeviceIdType.MESH
CHUNKS = 4


def kernel(
    sp_size, tok, wq, wk, wv, wo, gate, out,
    x, wqv, wkv, wvv, wov, gv, kv, qt, top, tot, acc, att, pf, own,
    s_near, s_far, s_own, r_near, r_far, r_own,
    load, tok_s, tok_r, far_s, far_r, fwd_s, fwd_r,
    z_s, x_s, kv_r, o_s, o_r,
):
    f32, bf16 = jnp.float32, jnp.bfloat16
    rows = tok.shape[0]
    half = 2 * rows
    block = 2 * half
    heads = wq.shape[1] // HD
    sp = lax.axis_index("sp")
    t = lax.axis_index("tp")
    core = lax.rem(t, 2)
    p = t // 2
    t1 = t + 1 - 2 * core
    t2 = lax.rem(t + 2, 4)
    r = sp // 2
    c = lax.rem(sp, 2)
    last_row = sp_size // 2 - 1
    spx = sp + 1 - 2 * c
    has_next = r < last_row
    pa, pb = p, 1 - p

    def at(n, unit):
        return pl.ds(pl.multiple_of(n * unit, unit), unit)

    loads = [
        pltpu.make_async_copy(tok, x.at[at(t, rows)], load.at[0]),
        pltpu.make_async_copy(gate, gv, load.at[1]),
        pltpu.make_async_copy(wk, wkv, load.at[2]),
        pltpu.make_async_copy(wv, wvv, load.at[3]),
        pltpu.make_async_copy(wq, wqv, load.at[4]),
        pltpu.make_async_copy(wo, wov, load.at[5]),
    ]
    for copy in loads:
        copy.start()

    barrier = pltpu.get_barrier_semaphore()
    pl.semaphore_signal(barrier, inc=1, device_id={"tp": t1}, device_id_type=MESH)
    pl.semaphore_signal(barrier, inc=1, device_id={"tp": t2}, device_id_type=MESH)
    pl.semaphore_signal(barrier, inc=1, device_id={"sp": spx}, device_id_type=MESH)

    @pl.when(has_next)
    def _():
        pl.semaphore_signal(barrier, inc=1, device_id={"sp": sp + 2}, device_id_type=MESH)

    @pl.when(r > 0)
    def _():
        pl.semaphore_signal(barrier, inc=1, device_id={"sp": sp - 2}, device_id_type=MESH)

    peers = 3 + jnp.where(has_next, 1, 0) + jnp.where(r > 0, 1, 0)
    pl.semaphore_wait(barrier, peers)

    step = rows // CHUNKS

    def piece(shard, n):
        return pl.ds(pl.multiple_of(shard * rows + n * step, step), step)

    def remote(src, dst, ss, rs, **where):
        return pltpu.make_async_remote_copy(
            src_ref=src, dst_ref=dst, send_sem=ss, recv_sem=rs,
            device_id=where, device_id_type=MESH,
        )

    far = []
    for n in range(CHUNKS):
        cp = remote(tok.at[pl.ds(n * step, step)], x.at[piece(t, n)], far_s.at[n], far_r.at[n], tp=t2)
        cp.start()
        far.append(cp)
    near = remote(tok, x.at[at(t, rows)], tok_s.at[0], tok_r.at[0], tp=t1)
    near.start()

    loads[1].wait()
    g = gv[...]
    hi = g.astype(bf16).astype(f32)
    mid = (g - hi).astype(bf16).astype(f32)
    low = (g - hi - mid).astype(bf16).astype(f32)
    parts = (hi, mid, low)
    extra = kv.shape[2] - 2 * HD
    index = lax.broadcasted_iota(jnp.int32, (extra, block), 0)
    key_side = jnp.where((index >= 3 * heads) & (index < 3 * heads + 3), 1.0, 0.0).astype(f32)
    for k in range(3):
        for h in range(heads):
            key_side = jnp.where(index == k * heads + h, -parts[k][h : h + 1, :], key_side)
    key_side = key_side.astype(bf16)
    kv[sp, 0, HD : HD + extra, :] = key_side[:, :half]
    kv[sp, 1, HD : HD + extra, :] = key_side[:, half:]
    for h in range(heads):
        side = jnp.where((index < 3 * heads) & (lax.rem(index, heads) == h), 1.0, 0.0).astype(f32)
        for k in range(3):
            side = jnp.where(index == 3 * heads + k, parts[k][h : h + 1, :], side)
        qt[h, HD : HD + extra, :] = side.astype(bf16)

    def project_kv(which):
        xs = x[at(which, half), :]
        key = jnp.dot(xs, wkv[...], preferred_element_type=f32)
        val = jnp.dot(xs, wvv[...], preferred_element_type=f32)
        both = jnp.concatenate([key, val], axis=1).T.astype(bf16)
        kv[sp, which, 0:HD, :] = both[:HD]
        kv[sp, which, HD + extra :, :] = both[HD:]

    def project_q(which):
        xs = x[at(which, half), :]
        q = jnp.dot(xs, wqv[...], preferred_element_type=f32).astype(bf16).astype(f32)
        q = (q * (float(HD) ** -0.5)).T.astype(bf16)
        for h in range(heads):
            qt[h, 0:HD, at(which, half)] = q[h * HD : (h + 1) * HD]

    def along(src, which):
        ref = kv.at[src, which]
        return remote(ref, ref, z_s.at[src // 2, which], kv_r.at[src, which], sp=sp + 2)

    def across(src, which):
        ref = kv.at[src, which]
        return remote(ref, ref, x_s.at[src // 2, which], kv_r.at[src, which], sp=spx)

    def send_own(which):
        @pl.when(has_next)
        def _():
            along(sp, which).start()

        @pl.when(c == 0)
        def _():
            across(sp, which).start()

    def relay(i, which):
        src = sp - 2 * i
        along(src, which).wait_recv()

        @pl.when(has_next)
        def _():
            along(src, which).start()

        across(src, which).start()

    loads[0].wait()
    loads[2].wait()
    loads[3].wait()
    near.wait_recv()
    project_kv(pa)
    send_own(pa)
    loads[4].wait()
    project_q(pa)

    fwd = []
    for n in range(CHUNKS):
        far[n].wait_recv()
        ref = x.at[piece(t2, n)]
        cp = remote(ref, ref, fwd_s.at[n], fwd_r.at[n], tp=t1)
        cp.start()
        fwd.append(cp)

        @pl.when(r >= n + 1)
        def _(n=n):
            relay(n + 1, pa)

    @pl.loop(CHUNKS + 1, r + 1)
    def _(i):
        relay(i, pa)

    for n in range(CHUNKS):
        fwd[n].wait_recv()
    project_kv(pb)
    send_own(pb)
    project_q(pb)

    def attend(src, diagonal):
        kt = jnp.concatenate([kv[src, 0, 0 : HD + extra, :], kv[src, 1, 0 : HD + extra, :]], axis=1)
        vt = jnp.concatenate([kv[src, 0, HD + extra :, :], kv[src, 1, HD + extra :, :]], axis=1)
        for h in range(heads):
            s = lax.dot_general(kt, qt[h], (((0,), (0,)), ((), ())), preferred_element_type=f32)
            lanes = slice(h * HD, (h + 1) * HD)
            if diagonal:
                key_pos = lax.broadcasted_iota(jnp.int32, s.shape, 0)
                query_pos = lax.broadcasted_iota(jnp.int32, s.shape, 1)
                s = jnp.where(key_pos <= query_pos, s, -jnp.inf)
                peak = jnp.max(s, axis=0, keepdims=True)
                w = jnp.exp(s - peak)
                tot[h : h + 1, :] = jnp.sum(w, axis=0, keepdims=True)
                acc[lanes, :] = jnp.dot(vt, w.astype(bf16), preferred_element_type=f32)
            else:
                before = top[h : h + 1, :]
                peak = jnp.maximum(before, jnp.max(s, axis=0, keepdims=True))
                w = jnp.exp(s - peak)
                decay = jnp.exp(before - peak)
                tot[h : h + 1, :] = tot[h : h + 1, :] * decay + jnp.sum(w, axis=0, keepdims=True)
                acc[lanes, :] = acc[lanes, :] * decay + jnp.dot(
                    vt, w.astype(bf16), preferred_element_type=f32
                )
            top[h : h + 1, :] = peak

    attend(sp, True)

    def wait_across(src):
        for which in (pa, pb):
            across(src, which).wait_recv()

    @pl.when(c == 1)
    def _():
        wait_across(spx)
        attend(spx, False)

    @pl.loop(1, r + 1)
    def _(i):
        relay(i, pb)
        attend(sp - 2 * i, False)
        wait_across(spx - 2 * i)
        attend(spx - 2 * i, False)

    for h in range(heads):
        lanes = slice(h * HD, (h + 1) * HD)
        acc[lanes, :] = acc[lanes, :] / tot[h : h + 1, :]
    att[...] = acc[...].T.astype(bf16)
    loads[5].wait()
    width = wo.shape[1] // CHUNKS
    near_sum, far_sum, own_sum = [], [], []
    for n in range(CHUNKS):
        cols = slice(n * width, (n + 1) * width)
        pf[:, cols] = jnp.dot(att[at(pb, half), :], wov[:, cols], preferred_element_type=f32)
        s_near[n] = pf[at(1 - core, rows), cols].astype(bf16)
        cp = remote(s_near.at[n], r_near.at[n], o_s.at[0, n], o_r.at[0, n], tp=t1)
        cp.start()
        near_sum.append(cp)
    for n in range(CHUNKS):
        cols = slice(n * width, (n + 1) * width)
        near_sum[n].wait_recv()
        s_far[n] = (pf[at(core, rows), cols] + r_near[n].astype(f32)).astype(bf16)
        cp = remote(s_far.at[n], r_far.at[n], o_s.at[1, n], o_r.at[1, n], tp=t2)
        cp.start()
        far_sum.append(cp)
    for n in range(CHUNKS):
        cols = slice(n * width, (n + 1) * width)
        own[:, cols] = jnp.dot(att[at(pa, half), :], wov[:, cols], preferred_element_type=f32)
        s_own[n] = own[at(1 - core, rows), cols].astype(bf16)
        cp = remote(s_own.at[n], r_own.at[n], o_s.at[2, n], o_r.at[2, n], tp=t1)
        cp.start()
        own_sum.append(cp)
    for n in range(CHUNKS):
        cols = slice(n * width, (n + 1) * width)
        own_sum[n].wait_recv()
        far_sum[n].wait_recv()
        total = own[at(core, rows), cols] + r_own[n].astype(f32) + r_far[n].astype(f32)
        out[:, cols] = total.astype(bf16)

    near.wait_send()
    for cp in far + fwd + near_sum + far_sum + own_sum:
        cp.wait_send()
    for which in (pa, pb):

        @pl.when(c == 0)
        def _(which=which):
            across(sp, which).wait_send()

        @pl.when(has_next)
        def _(which=which):
            along(sp, which).wait_send()

            @pl.loop(1, r + 1)
            def _(i):
                along(sp - 2 * i, which).wait_send()

        @pl.loop(1, r + 1)
        def _(i, which=which):
            across(sp - 2 * i, which).wait_send()


def per_device(sp_size, tokens, w_query, w_key, w_value, w_out, cum_gate):
    rows, width = tokens.shape
    half, block = 2 * rows, 4 * rows
    heads = w_query.shape[1] // HD
    out_width = w_out.shape[1]
    extra = -(-(3 * heads + 3) // 16) * 16
    bf16, f32 = jnp.bfloat16, jnp.float32
    dma = pltpu.SemaphoreType.DMA
    anywhere = pl.BlockSpec(memory_space=pl.ANY)
    part = pltpu.VMEM((CHUNKS, rows, out_width // CHUNKS), bf16)
    return pl.pallas_call(
        functools.partial(kernel, sp_size),
        out_shape=jax.ShapeDtypeStruct((rows, out_width), bf16),
        in_specs=[anywhere] * 6,
        out_specs=pl.BlockSpec(memory_space=pltpu.VMEM),
        scratch_shapes=[
            pltpu.VMEM((block, width), bf16),
            pltpu.VMEM(w_query.shape, bf16),
            pltpu.VMEM(w_key.shape, bf16),
            pltpu.VMEM(w_value.shape, bf16),
            pltpu.VMEM(w_out.shape, bf16),
            pltpu.VMEM(cum_gate.shape, f32),
            pltpu.VMEM((sp_size, 2, 2 * HD + extra, half), bf16),
            pltpu.VMEM((heads, HD + extra, block), bf16),
            pltpu.VMEM((heads, block), f32),
            pltpu.VMEM((heads, block), f32),
            pltpu.VMEM((heads * HD, block), f32),
            pltpu.VMEM((block, heads * HD), bf16),
            pltpu.VMEM((half, out_width), f32),
            pltpu.VMEM((half, out_width), f32),
            part, part, part, part, part, part,
            dma((6,)),
            dma((1,)), dma((1,)),
            dma((CHUNKS,)), dma((CHUNKS,)),
            dma((CHUNKS,)), dma((CHUNKS,)),
            dma((sp_size // 2, 2)), dma((sp_size // 2, 2)), dma((sp_size, 2)),
            dma((3, CHUNKS)), dma((3, CHUNKS)),
        ],
        compiler_params=pltpu.CompilerParams(
            collective_id=0, has_side_effects=True, vmem_limit_bytes=48 * 1024 * 1024
        ),
    )(tokens, w_query, w_key, w_value, w_out, cum_gate)


def solution(mesh):
    placed = (
        P(("sp", "tp"), None),
        P(None, "tp"),
        P(None, "tp"),
        P(None, "tp"),
        P("tp", None),
        P("tp", "sp"),
    )
    return jax.shard_map(
        functools.partial(per_device, mesh.shape["sp"]),
        mesh=mesh, in_specs=placed, out_specs=P(("sp", "tp"), None), check_vma=False,
    )
```

time: 112 us -> 43.3 us (0.39)
  the two profiles are of different devices: /device:TPU:26 before, /device:TPU:25 now
where the time goes in v1:
time: 43.3 us; the launch traced here: 43.1 us
  Pallas kernels  38.5 us (89%)
  local copies, waits for them, and re-layouts  4.51 us (10%)
    pallas_call x1, Pallas kernels, per_device(): pl.pallas_call(functools.partial(kernel, sp_size), out_shape=jax.ShapeDty...  38.5 us
    unnamed x11, local copies, waits for them, and re-layouts  4.51 us

profile of v1, /device:TPU:25, one launch (start us, length us, event | category | flops | bytes accessed | tf_op | source)
XLA Modules:
  0.0 43.1 jit_solution(3822319779448497550)
XLA Ops:
  0.0 0.0 copy-start
  0.0 1.3 %copy.7.wk = bf16[2048,64]{1,0:T(8,128)(2,1)S(1)} copy(bf16[2048,64]{0,1:T(8,128)(2,1)} %param.8) | data formatting | bytes 524288 | tf_op args[2]
  1.3 0.0 copy-start.2
  1.3 0.0 copy-start.3
  1.3 1.3 %copy.8.wv = bf16[2048,64]{1,0:T(8,128)(2,1)S(1)} copy(bf16[2048,64]{0,1:T(8,128)(2,1)} %param.9) | data formatting | bytes 524288 | tf_op args[3]
  2.6 0.0 copy-done
  2.6 0.0 copy-done.2
  2.6 0.0 copy-done.3
  2.6 0.0 copy-start.1
  2.7 1.2 %copy-done.1 = bf16[256,2048]{1,0:T(8,128)(2,1)S(1)} copy-done((bf16[256,2048]{1,0:T(8,128)(2,1)S(1)}, bf16[256,2048]{1,0:T(8,128)(2,1)}, u32[]{:S(2)}) %copy-start.1) | copy-done | bytes 1048600
  3.9 38.5 %shard_map.64 = bf16[64,2048]{1,0:T(8,128)(2,1)S(1)} custom-call(bf16[64,2048]{1,0:T(8,128)(2,1)S(1)} %copy-done.2, bf16[2048,256]{1,0:T(8,128)(2,1)S(1)} %copy-done, bf16[2048,64]{1,0:T(8,128)(2,1)S(1)} %copy.7.wk, bf16[2048,64]{1,0:T(8,128)(2,1)S(1)} %copy.8.wv, bf16[256,2048]{1,0:T(8,128)(2,1)S(1)} %copy-done.1, f32[4,256]{1,0:T(4,128)S(1)} %copy-done.3), custom_call_target="tpu_custom_call" | custom-call | tf_op jit(solution)/shard_map/pallas_call | solution.py:293
  42.4 0.7 %copy.10 = bf16[64,2048]{1,0:T(8,128)(2,1)} copy(bf16[64,2048]{1,0:T(8,128)(2,1)S(1)} %shard_map.64) | data formatting | bytes 524288
Async XLA Ops:
  0.0 2.6 %copy-start = (bf16[2048,256]{1,0:T(8,128)(2,1)S(1)}, bf16[2048,256]{1,0:T(8,128)(2,1)}, u32[]{:S(2)}) copy-start(bf16[2048,256]{1,0:T(8,128)(2,1)} %wq.1) | copy-start | bytes 3145732
  1.3 1.3 %copy-start.2 = (bf16[64,2048]{1,0:T(8,128)(2,1)S(1)}, bf16[64,2048]{1,0:T(8,128)(2,1)}, u32[]{:S(2)}) copy-start(bf16[64,2048]{1,0:T(8,128)(2,1)} %tok.1) | copy-start | bytes 786436
  1.3 1.3 %copy-start.3 = (f32[4,256]{1,0:T(4,128)S(1)}, f32[4,256]{1,0:T(4,128)}, u32[]{:S(2)}) copy-start(f32[4,256]{1,0:T(4,128)} %gate.1) | copy-start | bytes 12292
  2.6 1.2 %copy-start.1 = (bf16[256,2048]{1,0:T(8,128)(2,1)S(1)}, bf16[256,2048]{1,0:T(8,128)(2,1)}, u32[]{:S(2)}) copy-start(bf16[256,2048]{1,0:T(8,128)(2,1)} %wo.1) | copy-start | bytes 3145732

commit v2 on v1

--- a/solution.py
+++ b/solution.py
@@ -14,10 +14,10 @@
 
 def kernel(
     sp_size, tok, wq, wk, wv, wo, gate, out,
-    x, wqv, wkv, wvv, wov, gv, kv, qt, top, tot, acc, att, pf, own,
+    x, wqv, wkv, wvv, wboth, wov, gv, kv, qt, top, tot, acc, att, pf, own,
     s_near, s_far, s_own, r_near, r_far, r_own,
     load, tok_s, tok_r, far_s, far_r, fwd_s, fwd_r,
-    z_s, x_s, kv_r, o_s, o_r,
+    z_s, x_s, kv_r, o_s, o_r, ready,
 ):
     f32, bf16 = jnp.float32, jnp.bfloat16
     rows = tok.shape[0]
@@ -85,6 +85,18 @@
         far.append(cp)
     near = remote(tok, x.at[at(t, rows)], tok_s.at[0], tok_r.at[0], tp=t1)
     near.start()
+
+    @pl.when(has_next)
+    def _():
+        pl.semaphore_wait(ready, 1)
+
+    @pl.when(r > 0)
+    def _():
+        pl.semaphore_signal(ready, inc=1, device_id={"sp": sp - 2}, device_id_type=MESH)
+
+    loads[2].wait()
+    loads[3].wait()
+    wboth[...] = jnp.concatenate([wkv[...], wvv[...]], axis=1)
 
     loads[1].wait()
     g = gv[...]
@@ -109,9 +121,7 @@
 
     def project_kv(which):
         xs = x[at(which, half), :]
-        key = jnp.dot(xs, wkv[...], preferred_element_type=f32)
-        val = jnp.dot(xs, wvv[...], preferred_element_type=f32)
-        both = jnp.concatenate([key, val], axis=1).T.astype(bf16)
+        both = jnp.dot(xs, wboth[...], preferred_element_type=f32).T.astype(bf16)
         kv[sp, which, 0:HD, :] = both[:HD]
         kv[sp, which, HD + extra :, :] = both[HD:]
 
@@ -122,36 +132,30 @@
         for h in range(heads):
             qt[h, 0:HD, at(which, half)] = q[h * HD : (h + 1) * HD]
 
-    def along(src, which):
+    def along(src, which, row):
         ref = kv.at[src, which]
-        return remote(ref, ref, z_s.at[src // 2, which], kv_r.at[src, which], sp=sp + 2)
+        return remote(ref, ref, z_s.at[row, which], kv_r.at[src, which], sp=2 * row + c)
 
     def across(src, which):
         ref = kv.at[src, which]
         return remote(ref, ref, x_s.at[src // 2, which], kv_r.at[src, which], sp=spx)
 
     def send_own(which):
-        @pl.when(has_next)
-        def _():
-            along(sp, which).start()
+        @pl.loop(0, last_row - r)
+        def _(i):
+            along(sp, which, last_row - i).start()
 
         @pl.when(c == 0)
         def _():
             across(sp, which).start()
 
-    def relay(i, which):
-        src = sp - 2 * i
-        along(src, which).wait_recv()
-
-        @pl.when(has_next)
-        def _():
-            along(src, which).start()
-
-        across(src, which).start()
+    def relay(which):
+        @pl.loop(1, r + 1)
+        def _(i):
+            across(sp - 2 * i, which).wait_recv()
+            across(sp - 2 * i, which).start()
 
     loads[0].wait()
-    loads[2].wait()
-    loads[3].wait()
     near.wait_recv()
     project_kv(pa)
     send_own(pa)
@@ -166,18 +170,11 @@
         cp.start()
         fwd.append(cp)
 
-        @pl.when(r >= n + 1)
-        def _(n=n):
-            relay(n + 1, pa)
-
-    @pl.loop(CHUNKS + 1, r + 1)
-    def _(i):
-        relay(i, pa)
-
     for n in range(CHUNKS):
         fwd[n].wait_recv()
     project_kv(pb)
     send_own(pb)
+    relay(pa)
     project_q(pb)
 
     def attend(src, diagonal):
@@ -216,10 +213,14 @@
         wait_across(spx)
         attend(spx, False)
 
+    relay(pb)
+
     @pl.loop(1, r + 1)
     def _(i):
-        relay(i, pb)
         attend(sp - 2 * i, False)
+
+    @pl.loop(1, r + 1)
+    def _(i):
         wait_across(spx - 2 * i)
         attend(spx - 2 * i, False)
 
@@ -267,13 +268,9 @@
         def _(which=which):
             across(sp, which).wait_send()
 
-        @pl.when(has_next)
-        def _(which=which):
-            along(sp, which).wait_send()
-
-            @pl.loop(1, r + 1)
-            def _(i):
-                along(sp - 2 * i, which).wait_send()
+        @pl.loop(0, last_row - r)
+        def _(i, which=which):
+            along(sp, which, last_row - i).wait_send()
 
         @pl.loop(1, r + 1)
         def _(i, which=which):
@@ -300,6 +297,7 @@
             pltpu.VMEM(w_query.shape, bf16),
             pltpu.VMEM(w_key.shape, bf16),
             pltpu.VMEM(w_value.shape, bf16),
+            pltpu.VMEM((width, 2 * HD), bf16),
             pltpu.VMEM(w_out.shape, bf16),
             pltpu.VMEM(cum_gate.shape, f32),
             pltpu.VMEM((sp_size, 2, 2 * HD + extra, half), bf16),
@@ -317,6 +315,7 @@
             dma((CHUNKS,)), dma((CHUNKS,)),
             dma((sp_size // 2, 2)), dma((sp_size // 2, 2)), dma((sp_size, 2)),
             dma((3, CHUNKS)), dma((3, CHUNKS)),
+            pltpu.SemaphoreType.REGULAR,
         ],
         compiler_params=pltpu.CompilerParams(
             collective_id=0, has_side_effects=True, vmem_limit_bytes=48 * 1024 * 1024

time: 43.3 us -> 35.5 us (0.82)
  the two profiles are of different devices: /device:TPU:25 before, /device:TPU:26 now
where the time goes in v2:
time: 35.5 us; the launch traced here: 35.3 us
  Pallas kernels  30.7 us (86%)
  local copies, waits for them, and re-layouts  4.51 us (13%)
    pallas_call x1, Pallas kernels, per_device(): pl.pallas_call(functools.partial(kernel, sp_size), out_shape=jax.ShapeDty...  30.7 us
    unnamed x11, local copies, waits for them, and re-layouts  4.51 us

profile of v2, /device:TPU:26, one launch (start us, length us, event | category | flops | bytes accessed | tf_op | source)
XLA Modules:
  0.0 35.3 jit_solution(6020116427679899680)
XLA Ops:
  0.0 0.0 copy-start
  0.0 1.3 %copy.7.wk = bf16[2048,64]{1,0:T(8,128)(2,1)S(1)} copy(bf16[2048,64]{0,1:T(8,128)(2,1)} %param.8) | data formatting | bytes 524288 | tf_op args[2]
  1.3 0.0 copy-start.2
  1.3 0.0 copy-start.3
  1.3 1.3 %copy.8.wv = bf16[2048,64]{1,0:T(8,128)(2,1)S(1)} copy(bf16[2048,64]{0,1:T(8,128)(2,1)} %param.9) | data formatting | bytes 524288 | tf_op args[3]
  2.6 0.0 copy-done
  2.6 0.0 copy-done.2
  2.6 0.0 copy-done.3
  2.6 0.0 copy-start.1
  2.7 1.2 %copy-done.1 = bf16[256,2048]{1,0:T(8,128)(2,1)S(1)} copy-done((bf16[256,2048]{1,0:T(8,128)(2,1)S(1)}, bf16[256,2048]{1,0:T(8,128)(2,1)}, u32[]{:S(2)}) %copy-start.1) | copy-done | bytes 1048600
  3.9 30.7 %shard_map.64 = bf16[64,2048]{1,0:T(8,128)(2,1)S(1)} custom-call(bf16[64,2048]{1,0:T(8,128)(2,1)S(1)} %copy-done.2, bf16[2048,256]{1,0:T(8,128)(2,1)S(1)} %copy-done, bf16[2048,64]{1,0:T(8,128)(2,1)S(1)} %copy.7.wk, bf16[2048,64]{1,0:T(8,128)(2,1)S(1)} %copy.8.wv, bf16[256,2048]{1,0:T(8,128)(2,1)S(1)} %copy-done.1, f32[4,256]{1,0:T(4,128)S(1)} %copy-done.3), custom_call_target="tpu_custom_call" | custom-call | tf_op jit(solution)/shard_map/pallas_call | solution.py:290
  34.6 0.7 %copy.10 = bf16[64,2048]{1,0:T(8,128)(2,1)} copy(bf16[64,2048]{1,0:T(8,128)(2,1)S(1)} %shard_map.64) | data formatting | bytes 524288
Async XLA Ops:
  0.0 2.6 %copy-start = (bf16[2048,256]{1,0:T(8,128)(2,1)S(1)}, bf16[2048,256]{1,0:T(8,128)(2,1)}, u32[]{:S(2)}) copy-start(bf16[2048,256]{1,0:T(8,128)(2,1)} %wq.1) | copy-start | bytes 3145732
  1.3 1.3 %copy-start.2 = (bf16[64,2048]{1,0:T(8,128)(2,1)S(1)}, bf16[64,2048]{1,0:T(8,128)(2,1)}, u32[]{:S(2)}) copy-start(bf16[64,2048]{1,0:T(8,128)(2,1)} %tok.1) | copy-start | bytes 786436
  1.3 1.3 %copy-start.3 = (f32[4,256]{1,0:T(4,128)S(1)}, f32[4,256]{1,0:T(4,128)}, u32[]{:S(2)}) copy-start(f32[4,256]{1,0:T(4,128)} %gate.1) | copy-start | bytes 12292
  2.6 1.2 %copy-start.1 = (bf16[256,2048]{1,0:T(8,128)(2,1)S(1)}, bf16[256,2048]{1,0:T(8,128)(2,1)}, u32[]{:S(2)}) copy-start(bf16[256,2048]{1,0:T(8,128)(2,1)} %wo.1) | copy-start | bytes 3145732

commit v3 on v2

--- a/solution.py
+++ b/solution.py
@@ -14,7 +14,7 @@
 
 def kernel(
     sp_size, tok, wq, wk, wv, wo, gate, out,
-    x, wqv, wkv, wvv, wboth, wov, gv, kv, qt, top, tot, acc, att, pf, own,
+    x, wqv, wboth, wov, gv, kv, qt, top, tot, acc, att, pf, own,
     s_near, s_far, s_own, r_near, r_far, r_own,
     load, tok_s, tok_r, far_s, far_r, fwd_s, fwd_r,
     z_s, x_s, kv_r, o_s, o_r, ready,
@@ -43,8 +43,8 @@
     loads = [
         pltpu.make_async_copy(tok, x.at[at(t, rows)], load.at[0]),
         pltpu.make_async_copy(gate, gv, load.at[1]),
-        pltpu.make_async_copy(wk, wkv, load.at[2]),
-        pltpu.make_async_copy(wv, wvv, load.at[3]),
+        pltpu.make_async_copy(wk, wboth.at[0:HD], load.at[2]),
+        pltpu.make_async_copy(wv, wboth.at[HD : 2 * HD], load.at[3]),
         pltpu.make_async_copy(wq, wqv, load.at[4]),
         pltpu.make_async_copy(wo, wov, load.at[5]),
     ]
@@ -85,18 +85,6 @@
         far.append(cp)
     near = remote(tok, x.at[at(t, rows)], tok_s.at[0], tok_r.at[0], tp=t1)
     near.start()
-
-    @pl.when(has_next)
-    def _():
-        pl.semaphore_wait(ready, 1)
-
-    @pl.when(r > 0)
-    def _():
-        pl.semaphore_signal(ready, inc=1, device_id={"sp": sp - 2}, device_id_type=MESH)
-
-    loads[2].wait()
-    loads[3].wait()
-    wboth[...] = jnp.concatenate([wkv[...], wvv[...]], axis=1)
 
     loads[1].wait()
     g = gv[...]
@@ -121,7 +109,9 @@
 
     def project_kv(which):
         xs = x[at(which, half), :]
-        both = jnp.dot(xs, wboth[...], preferred_element_type=f32).T.astype(bf16)
+        both = lax.dot_general(
+            wboth[...], xs, (((1,), (1,)), ((), ())), preferred_element_type=f32
+        ).astype(bf16)
         kv[sp, which, 0:HD, :] = both[:HD]
         kv[sp, which, HD + extra :, :] = both[HD:]
 
@@ -155,9 +145,29 @@
             across(sp - 2 * i, which).wait_recv()
             across(sp - 2 * i, which).start()
 
+    def hear():
+        @pl.when(r < last_row - 1)
+        def _():
+            pl.semaphore_wait(ready, 1)
+
+    @pl.when(r > 0)
+    def _():
+        hear()
+
+        @pl.when(has_next)
+        def _():
+            pl.semaphore_signal(ready, inc=1, device_id={"sp": sp - 2}, device_id_type=MESH)
+
     loads[0].wait()
+    loads[2].wait()
+    loads[3].wait()
     near.wait_recv()
     project_kv(pa)
+
+    @pl.when(r == 0)
+    def _():
+        hear()
+
     send_own(pa)
     loads[4].wait()
     project_q(pa)
@@ -295,9 +305,7 @@
         scratch_shapes=[
             pltpu.VMEM((block, width), bf16),
             pltpu.VMEM(w_query.shape, bf16),
-            pltpu.VMEM(w_key.shape, bf16),
-            pltpu.VMEM(w_value.shape, bf16),
-            pltpu.VMEM((width, 2 * HD), bf16),
+            pltpu.VMEM((2 * HD, width), bf16),
             pltpu.VMEM(w_out.shape, bf16),
             pltpu.VMEM(cum_gate.shape, f32),
             pltpu.VMEM((sp_size, 2, 2 * HD + extra, half), bf16),
@@ -318,9 +326,9 @@
             pltpu.SemaphoreType.REGULAR,
         ],
         compiler_params=pltpu.CompilerParams(
-            collective_id=0, has_side_effects=True, vmem_limit_bytes=48 * 1024 * 1024
+            collective_id=0, has_side_effects=True, vmem_limit_bytes=62 * 1024 * 1024
         ),
-    )(tokens, w_query, w_key, w_value, w_out, cum_gate)
+    )(tokens, w_query, w_key.T, w_value.T, w_out, cum_gate)
 
 
 def solution(mesh):

time: 35.5 us -> 33.1 us (0.932)
  local copies, waits for them, and re-layouts: 4.51 us -> 1.67 us
  Pallas kernels: 30.7 us -> 31.3 us
    unnamed x11 -> x1, local copies, waits for them, and re-layouts: 4.51 us -> 1.67 us
    pallas_call x1, Pallas kernels: 30.7 us -> 31.3 us  [per_device(): pl.pallas_call(functools.partial(kernel, sp_size), out_shape=jax.ShapeDty...]
where the time goes in v3:
time: 33.1 us; the launch traced here: 33 us
  Pallas kernels  31.3 us (95%)
  local copies, waits for them, and re-layouts  1.67 us (5%)
    pallas_call x1, Pallas kernels, per_device(): pl.pallas_call(functools.partial(kernel, sp_size), out_shape=jax.ShapeDty...  31.3 us
    unnamed x1, local copies, waits for them, and re-layouts  1.67 us

profile of v3, /device:TPU:26, one launch (start us, length us, event | category | flops | bytes accessed | tf_op | source)
XLA Modules:
  0.0 33.0 jit_solution(6589281279696928313)
XLA Ops:
  0.0 31.3 %shard_map.64 = bf16[64,2048]{1,0:T(8,128)(2,1)} custom-call(bf16[64,2048]{1,0:T(8,128)(2,1)} %tok.1, bf16[2048,256]{1,0:T(8,128)(2,1)} %wq.1, bf16[64,2048]{1,0:T(8,128)(2,1)} %bitcast.2, bf16[64,2048]{1,0:T(8,128)(2,1)} %bitcast.3, bf16[256,2048]{1,0:T(8,128)(2,1)} %wo.1, f32[4,256]{1,0:T(4,128)} %gate.1), custom_call_target="tpu_custom_call" | custom-call | tf_op jit(solution)/shard_map/pallas_call | solution.py:300
  31.3 1.7 %copy.8 = bf16[64,2048]{1,0:T(8,128)(2,1)} copy(bf16[64,2048]{1,0:T(8,128)(2,1)} %shard_map.64) | data formatting | bytes 524288

commit v4 on v3

--- a/solution.py
+++ b/solution.py
@@ -18,6 +18,7 @@
     s_near, s_far, s_own, r_near, r_far, r_own,
     load, tok_s, tok_r, far_s, far_r, fwd_s, fwd_r,
     z_s, x_s, kv_r, o_s, o_r, ready,
+    wg, ag, w_s, w_r, a_s, a_r,
 ):
     f32, bf16 = jnp.float32, jnp.bfloat16
     rows = tok.shape[0]
@@ -30,6 +31,7 @@
     p = t // 2
     t1 = t + 1 - 2 * core
     t2 = lax.rem(t + 2, 4)
+    t3 = 3 - t
     r = sp // 2
     c = lax.rem(sp, 2)
     last_row = sp_size // 2 - 1
@@ -54,6 +56,7 @@
     barrier = pltpu.get_barrier_semaphore()
     pl.semaphore_signal(barrier, inc=1, device_id={"tp": t1}, device_id_type=MESH)
     pl.semaphore_signal(barrier, inc=1, device_id={"tp": t2}, device_id_type=MESH)
+    pl.semaphore_signal(barrier, inc=1, device_id={"tp": t3}, device_id_type=MESH)
     pl.semaphore_signal(barrier, inc=1, device_id={"sp": spx}, device_id_type=MESH)
 
     @pl.when(has_next)
@@ -64,7 +67,7 @@
     def _():
         pl.semaphore_signal(barrier, inc=1, device_id={"sp": sp - 2}, device_id_type=MESH)
 
-    peers = 3 + jnp.where(has_next, 1, 0) + jnp.where(r > 0, 1, 0)
+    peers = 4 + jnp.where(has_next, 1, 0) + jnp.where(r > 0, 1, 0)
     pl.semaphore_wait(barrier, peers)
 
     step = rows // CHUNKS
@@ -180,8 +183,16 @@
         cp.start()
         fwd.append(cp)
 
+    loads[5].wait()
+    split = wo.shape[1] // 2
+    gathered = pl.ds(0, split)
+    w_far = remote(wov.at[:, gathered], wg.at[t], w_s.at[1], w_r.at[1], tp=t2)
+    w_near = remote(wov.at[:, gathered], wg.at[t], w_s.at[0], w_r.at[0], tp=t1)
+    w_far.start()
+
     for n in range(CHUNKS):
         fwd[n].wait_recv()
+    w_near.start()
     project_kv(pb)
     send_own(pb)
     relay(pa)
@@ -238,39 +249,53 @@
         lanes = slice(h * HD, (h + 1) * HD)
         acc[lanes, :] = acc[lanes, :] / tot[h : h + 1, :]
     att[...] = acc[...].T.astype(bf16)
-    loads[5].wait()
-    width = wo.shape[1] // CHUNKS
+    exchange = []
+    for n, peer in ((1, t2), (2, t3), (0, t1)):
+        cp = remote(att.at[at(peer, rows)], ag.at[t], a_s.at[n], a_r.at[n], tp=peer)
+        cp.start()
+        exchange.append(cp)
+    width = (wo.shape[1] - split) // CHUNKS
     near_sum, far_sum, own_sum = [], [], []
     for n in range(CHUNKS):
-        cols = slice(n * width, (n + 1) * width)
+        cols = slice(split + n * width, split + (n + 1) * width)
         pf[:, cols] = jnp.dot(att[at(pb, half), :], wov[:, cols], preferred_element_type=f32)
         s_near[n] = pf[at(1 - core, rows), cols].astype(bf16)
         cp = remote(s_near.at[n], r_near.at[n], o_s.at[0, n], o_r.at[0, n], tp=t1)
         cp.start()
         near_sum.append(cp)
     for n in range(CHUNKS):
-        cols = slice(n * width, (n + 1) * width)
+        cols = slice(split + n * width, split + (n + 1) * width)
         near_sum[n].wait_recv()
         s_far[n] = (pf[at(core, rows), cols] + r_near[n].astype(f32)).astype(bf16)
         cp = remote(s_far.at[n], r_far.at[n], o_s.at[1, n], o_r.at[1, n], tp=t2)
         cp.start()
         far_sum.append(cp)
     for n in range(CHUNKS):
-        cols = slice(n * width, (n + 1) * width)
+        cols = slice(split + n * width, split + (n + 1) * width)
         own[:, cols] = jnp.dot(att[at(pa, half), :], wov[:, cols], preferred_element_type=f32)
         s_own[n] = own[at(1 - core, rows), cols].astype(bf16)
         cp = remote(s_own.at[n], r_own.at[n], o_s.at[2, n], o_r.at[2, n], tp=t1)
         cp.start()
         own_sum.append(cp)
-    for n in range(CHUNKS):
-        cols = slice(n * width, (n + 1) * width)
+
+    w_far.wait_recv()
+    w_fwd = remote(wg.at[t2], wg.at[t2], w_s.at[2], w_r.at[2], tp=t1)
+    w_fwd.start()
+    total = jnp.dot(att[at(t, rows), :], wov[:, gathered], preferred_element_type=f32)
+    for waits, peer in (((w_near, exchange[2]), t1), ((exchange[0],), t2), ((w_fwd, exchange[1]), t3)):
+        for cp in waits:
+            cp.wait_recv()
+        total = total + jnp.dot(ag[peer], wg[peer], preferred_element_type=f32)
+    out[:, gathered] = total.astype(bf16)
+    for n in range(CHUNKS):
+        cols = slice(split + n * width, split + (n + 1) * width)
         own_sum[n].wait_recv()
         far_sum[n].wait_recv()
         total = own[at(core, rows), cols] + r_own[n].astype(f32) + r_far[n].astype(f32)
         out[:, cols] = total.astype(bf16)
 
     near.wait_send()
-    for cp in far + fwd + near_sum + far_sum + own_sum:
+    for cp in far + fwd + near_sum + far_sum + own_sum + exchange + [w_far, w_near, w_fwd]:
         cp.wait_send()
     for which in (pa, pb):
 
@@ -296,7 +321,7 @@
     bf16, f32 = jnp.bfloat16, jnp.float32
     dma = pltpu.SemaphoreType.DMA
     anywhere = pl.BlockSpec(memory_space=pl.ANY)
-    part = pltpu.VMEM((CHUNKS, rows, out_width // CHUNKS), bf16)
+    part = pltpu.VMEM((CHUNKS, rows, out_width // 2 // CHUNKS), bf16)
     return pl.pallas_call(
         functools.partial(kernel, sp_size),
         out_shape=jax.ShapeDtypeStruct((rows, out_width), bf16),
@@ -324,6 +349,9 @@
             dma((sp_size // 2, 2)), dma((sp_size // 2, 2)), dma((sp_size, 2)),
             dma((3, CHUNKS)), dma((3, CHUNKS)),
             pltpu.SemaphoreType.REGULAR,
+            pltpu.VMEM((4, w_out.shape[0], out_width // 2), bf16),
+            pltpu.VMEM((4, rows, w_out.shape[0]), bf16),
+            dma((3,)), dma((3,)), dma((3,)), dma((3,)),
         ],
         compiler_params=pltpu.CompilerParams(
             collective_id=0, has_side_effects=True, vmem_limit_bytes=62 * 1024 * 1024

time: 33.1 us -> 31.6 us (0.955)
  Pallas kernels: 31.3 us -> 29.7 us
    pallas_call x1, Pallas kernels: 31.3 us -> 29.7 us  [per_device(): pl.pallas_call(functools.partial(kernel, sp_size), out_shape=jax.ShapeDty...]
where the time goes in v4:
time: 31.6 us; the launch traced here: 31.4 us
  Pallas kernels  29.7 us (94%)
  local copies, waits for them, and re-layouts  1.67 us (5%)
    pallas_call x1, Pallas kernels, per_device(): pl.pallas_call(functools.partial(kernel, sp_size), out_shape=jax.ShapeDty...  29.7 us
    unnamed x1, local copies, waits for them, and re-layouts  1.67 us

profile of v4, /device:TPU:26, one launch (start us, length us, event | category | flops | bytes accessed | tf_op | source)
XLA Modules:
  0.0 31.4 jit_solution(16922195504489282933)
XLA Ops:
  0.0 29.7 %shard_map.64 = bf16[64,2048]{1,0:T(8,128)(2,1)} custom-call(bf16[64,2048]{1,0:T(8,128)(2,1)} %tok.1, bf16[2048,256]{1,0:T(8,128)(2,1)} %wq.1, bf16[64,2048]{1,0:T(8,128)(2,1)} %bitcast.2, bf16[64,2048]{1,0:T(8,128)(2,1)} %bitcast.3, bf16[256,2048]{1,0:T(8,128)(2,1)} %wo.1, f32[4,256]{1,0:T(4,128)} %gate.1), custom_call_target="tpu_custom_call" | custom-call | tf_op jit(solution)/shard_map/pallas_call | solution.py:325
  29.7 1.7 %copy.8 = bf16[64,2048]{1,0:T(8,128)(2,1)} copy(bf16[64,2048]{1,0:T(8,128)(2,1)} %shard_map.64) | data formatting | bytes 524288
